TPU v7x, 32 devices: a whole 2x2x4 slice. The times are simulated.
32 devices in a mesh: rep: 2 (over y), fs: 4 (over z), tp: 4 (over x, core).
Axes of the slice: x: 2, y: 2, z: 4, core: 2. Of those that a mesh axis runs over, the one named last changes fastest.
Arguments:
- stream: bfloat16 [4096, 2048], P(('rep', 'fs', 'tp')), may hold values from -6 to 6
- gain_before: float32 [2048], replicated, may hold values from 0.1 to 1.9
- gain_after: float32 [2048], replicated, may hold values from 0.1 to 1.9
- proj_gate: bfloat16 [2048, 3584], P('fs', 'tp'), may hold values from -0.125 to 0.125
- proj_lift: bfloat16 [2048, 3584], P('fs', 'tp'), may hold values from -0.125 to 0.125
- proj_down: bfloat16 [3584, 2048], P('tp', 'fs'), may hold values from -0.09375 to 0.09375
- mixer_gain: float32 [2048], replicated, may hold values from 0.1 to 1.9
- mixer_u: bfloat16 [2048, 2048], P('fs', 'tp'), may hold values from -0.125 to 0.125
- mixer_v: bfloat16 [2048, 2048], P('fs', 'tp'), may hold values from -1 to 1
- layer_gain: float32 [2048], P('tp'), may hold values from 0.1 to 1.9
- layer_shift: float32 [2048], P('tp'), may hold values from -3 to 3
- spatial: bfloat16 [16, 128, 128], P('tp'), may hold values from -0.5 to 0.5
- spatial_shift: float32 [16, 128], P('tp'), may hold values from 0.2 to 2
- mixer_down: bfloat16 [2048, 2048], P('tp', 'fs'), may hold values from -0.125 to 0.125
Outputs:
- result: bfloat16 [4096, 2048], P(('rep', 'fs', 'tp'))
All inputs are finite; a program needn't handle non-finite values.
Results may differ from a plain program's by a relative error of at most 0.017.
Values may be sent and summed in bfloat16 or wider, within the bound.
A program may use at most 128 MiB of HBM per device.

v0:
```python
import jax
import jax.numpy as jnp
from jax import lax
from jax.sharding import PartitionSpec as P

GROUP_DIM = 128
SPAN = 128
A = 2048
norm_epsilon = 1e-06
layer_epsilon = 1e-05


def norm_rows(row_block, scale_gain):
    widened = row_block.astype(jnp.float32)
    factor = lax.rsqrt(jnp.mean(widened * widened, axis=1, keepdims=True) + norm_epsilon)
    return (widened * factor * scale_gain).astype(jnp.bfloat16)


def gathered_norm(stream_rows, scale_gain):
    gathered = lax.all_gather(stream_rows, "tp", axis=0, tiled=True)
    return norm_rows(gathered, scale_gain)


def pair_adder(normed, pieces):
    return (
        jnp.dot(normed, pieces[0], preferred_element_type=jnp.float32),
        jnp.dot(normed, pieces[1], preferred_element_type=jnp.float32),
    )


def activate(gate_vals, lift_vals):
    return (jax.nn.silu(gate_vals) * lift_vals).astype(jnp.bfloat16)


def half_again(stream_rows, scale_gain, proj_gate, proj_lift, proj_down):
    normed = gathered_norm(stream_rows, scale_gain)
    gate_vals, lift_vals = pair_adder(
        normed,
        (
            lax.all_gather(proj_gate, "fs", axis=0, tiled=True),
            lax.all_gather(proj_lift, "fs", axis=0, tiled=True),
        ),
    )
    hidden = activate(gate_vals, lift_vals)
    partial_value = jnp.dot(
        hidden,
        lax.all_gather(proj_down, "fs", axis=1, tiled=True),
        preferred_element_type=jnp.float32,
    )
    summed = lax.psum_scatter(
        partial_value.astype(jnp.bfloat16), "tp", scatter_dimension=0, tiled=True
    ).astype(jnp.float32)
    return (stream_rows.astype(jnp.float32) + 0.5 * summed).astype(jnp.bfloat16)


def token_mixer(
    stream_rows,
    mixer_gain,
    mixer_u,
    mixer_v,
    layer_gain,
    layer_shift,
    spatial,
    spatial_shift,
    mixer_down,
):
    gathered = lax.all_gather(stream_rows, "tp", axis=0, tiled=True)
    normed = norm_rows(gathered, mixer_gain)
    seq_tokens = normed.shape[0]
    u_vals, v_vals = pair_adder(
        normed,
        (
            lax.all_gather(mixer_u, "fs", axis=0, tiled=True),
            lax.all_gather(mixer_v, "fs", axis=0, tiled=True),
        ),
    )
    lifted = jax.nn.gelu(v_vals)
    moments = lax.psum((jnp.sum(lifted, axis=1), jnp.sum(lifted * lifted, axis=1)), "tp")
    centre = moments[0] / A
    spread = moments[1] / A - centre * centre
    normed_v = (
        (lifted - centre[:, None]) * lax.rsqrt(spread[:, None] + layer_epsilon) * layer_gain
        + layer_shift
    ).astype(jnp.bfloat16)
    groups_here = spatial.shape[0]
    blocked = normed_v.reshape(seq_tokens // SPAN, SPAN, groups_here, GROUP_DIM)
    causal = jnp.tril(jnp.ones((SPAN, SPAN), dtype=bool))
    masked = jnp.where(causal[None], spatial, jnp.zeros((), jnp.bfloat16))
    mixed_v = jnp.einsum("gts,bsgd->btgd", masked, blocked, preferred_element_type=jnp.float32)
    mixed_v = mixed_v + spatial_shift.T[None, :, :, None]
    gated = (jax.nn.gelu(u_vals) * mixed_v.reshape(seq_tokens, groups_here * GROUP_DIM)).astype(
        jnp.bfloat16
    )
    partial_value = jnp.dot(
        gated,
        lax.all_gather(mixer_down, "fs", axis=1, tiled=True),
        preferred_element_type=jnp.float32,
    )
    summed = lax.psum_scatter(
        partial_value.astype(jnp.bfloat16), "tp", scatter_dimension=0, tiled=True
    ).astype(jnp.float32)
    return (stream_rows.astype(jnp.float32) + summed).astype(jnp.bfloat16)


def body(
    stream,
    gain_before,
    gain_after,
    proj_gate,
    proj_lift,
    proj_down,
    mixer_gain,
    mixer_u,
    mixer_v,
    layer_gain,
    layer_shift,
    spatial,
    spatial_shift,
    mixer_down,
):
    first = half_again(stream, gain_before, proj_gate, proj_lift, proj_down)
    second = token_mixer(
        first,
        mixer_gain,
        mixer_u,
        mixer_v,
        layer_gain,
        layer_shift,
        spatial,
        spatial_shift,
        mixer_down,
    )
    result = half_again(second, gain_after, proj_gate, proj_lift, proj_down)
    return result


def solution(mesh):
    placed = (
        P(("rep", "fs", "tp"), None),
        P(),
        P(),
        P("fs", "tp"),
        P("fs", "tp"),
        P("tp", "fs"),
        P(),
        P("fs", "tp"),
        P("fs", "tp"),
        P("tp"),
        P("tp"),
        P("tp", None, None),
        P("tp", None),
        P("tp", "fs"),
    )
    return jax.shard_map(
        body, mesh=mesh, in_specs=placed, out_specs=P(("rep", "fs", "tp"), None), check_vma=False
    )
```

profile of v0, /device:TPU:0, one launch (start us, length us, event | category | flops | bytes accessed | tf_op | source)
XLA Modules:
  0.0 575.2 jit_solution(15976335767558670113)
XLA Ops:
  6.5 0.0 all-gather.10.cloned.1.call-start
  6.5 0.7 all-gather.10.cloned.1.call-update
  7.3 0.0 all-gather.12.cloned.1.call-start
  7.3 0.7 all-gather.12.cloned.1.call-update
  8.0 0.0 copy-start.10
  8.0 0.0 all-gather.14.cloned.1.call-start
  8.1 0.7 all-gather.14.cloned.1.call-update
  8.8 0.0 all-gather.16.cloned.1.call-start
  8.8 0.5 all-gather.16.cloned.1.call-update
  9.3 0.0 reduce-scatter.4.cloned.1.call-start
  9.4 24.8 %all-gather.10.cloned.1.call-done = bf16[512,2048]{1,0:T(8,128)(2,1)} async-done(((bf16[128,2048]{1,0:T(8,128)(2,1)}), bf16[512,2048]{1,0:T(8,128)(2,1)}) %all-gather.10.cloned.1.call-update) | async-done | bytes 2097168 | tf_op jit(solution)/shard_map/all_gather | solution.py:20
  34.2 2.2 fusion
  36.4 71.5 %all-gather.12.cloned.1.call-done = bf16[2048,896]{1,0:T(8,128)(2,1)} async-done(((bf16[512,896]{1,0:T(8,128)(2,1)}), bf16[2048,896]{1,0:T(8,128)(2,1)}) %all-gather.12.cloned.1.call-update) | async-done | bytes 3670032 | tf_op jit(solution)/shard_map/all_gather | solution.py:40
  107.9 0.0 copy-done.10
  107.9 0.0 copy-done.4
  107.9 5.6 fusion.42
  113.5 66.6 %all-gather.14.cloned.1.call-done = bf16[2048,896]{1,0:T(8,128)(2,1)} async-done(((bf16[512,896]{1,0:T(8,128)(2,1)}), bf16[2048,896]{1,0:T(8,128)(2,1)}) %all-gather.14.cloned.1.call-update) | async-done | bytes 3670032 | tf_op jit(solution)/shard_map/all_gather | solution.py:41
  180.2 72.1 %all-gather.16.cloned.1.call-done = bf16[896,2048]{1,0:T(8,128)(2,1)} async-done(((bf16[896,512]{1,0:T(8,128)(2,1)}), bf16[896,2048]{1,0:T(8,128)(2,1)}) %all-gather.16.cloned.1.call-update) | async-done | bytes 3670032 | tf_op jit(solution)/shard_map/all_gather | solution.py:47
  252.3 9.7 %convolution_convert_fusion.1 = bf16[512,2048]{1,0:T(8,128)(2,1)} fusion(bf16[896,2048]{1,0:T(8,128)(2,1)} %all-gather.16.cloned.1.call-done, f32[512,896]{1,0:T(8,128)} %fusion.42, bf16[2048,896]{1,0:T(8,128)(2,1)} %all-gather.14.cloned.1.call-done, bf16[512,2048]{1,0:T(8,128)(2,1)S(1)} %copy-done.4, f32[2048]{0:T(1024)S(1)} %copy-done.10, ...), kind=kOutput, calls=%fused_computation.16 | convolution fusion | flops 3766091776 | bytes 13379584 | tf_op jit(solution)/shard_map/dot_general | solution.py:45
  262.0 0.0 reduce-scatter.4.cloned.1.call-update
  262.0 0.0 all-gather.18.cloned.1.call-start
  262.0 29.9 %reduce-scatter.4.cloned.1.call-done = bf16[128,2048]{1,0:T(8,128)(2,1)} async-done(((bf16[512,2048]{1,0:T(8,128)(2,1)}), bf16[128,2048]{1,0:T(8,128)(2,1)}) %reduce-scatter.4.cloned.1.call-update) | async-done | bytes 524304 | tf_op jit(solution)/shard_map/reduce_scatter | solution.py:50
  291.9 0.0 copy-done.2
  291.9 2.0 add_convert_fusion.3
  293.9 0.0 all-gather.18.cloned.1.call-update
  293.9 0.0 all-gather.22.cloned.1.call-start
  294.0 0.7 all-gather.22.cloned.1.call-update
  294.7 0.0 all-gather.20.cloned.1.call-start
  294.7 0.7 all-gather.20.cloned.1.call-update
  295.4 0.0 all-gather.24.cloned.1.call-start
  295.5 0.7 all-gather.24.cloned.1.call-update
  296.2 0.0 reduce-scatter.6.cloned.1.call-start
  296.2 20.4 %all-gather.18.cloned.1.call-done = bf16[512,2048]{1,0:T(8,128)(2,1)} async-done(((bf16[128,2048]{1,0:T(8,128)(2,1)}), bf16[512,2048]{1,0:T(8,128)(2,1)}) %all-gather.18.cloned.1.call-update) | async-done | bytes 2097168 | tf_op jit(solution)/shard_map/all_gather | solution.py:67
  316.6 2.2 fusion.3
  318.9 0.0 copy-start.7
  318.9 0.0 copy-start.8
  318.9 45.0 %all-gather.22.cloned.1.call-done = bf16[2048,512]{1,0:T(8,128)(2,1)} async-done(((bf16[512,512]{1,0:T(8,128)(2,1)}), bf16[2048,512]{1,0:T(8,128)(2,1)}) %all-gather.22.cloned.1.call-update) | async-done | bytes 2097168 | tf_op jit(solution)/shard_map/all_gather | solution.py:74
  363.9 0.0 copy-done.11
  363.9 0.0 copy-done.3
  363.9 4.1 fusion.60
  368.0 6.5 %all-reduce = (f32[512]{0:T(512)S(1)}, f32[512]{0:T(512)S(1)}) all-reduce(f32[512]{0:T(512)S(1)} %get-tuple-element.6, f32[512]{0:T(512)S(1)} %get-tuple-element.5), channel_id=1, replica_groups=mesh['rep'=2,'fs'=4,'tp'=4] {'tp'}, use_global_device_ids=true, to_apply=%region_6.7 | all-reduce | flops 1024 | bytes 8192 | tf_op jit(solution)/shard_map/psum | solution.py:78
  374.6 1.5 add_convert_fusion.2
  376.0 0.9 reshape.47
  377.0 0.0 copy-done.9
  377.0 1.4 fusion.9
  378.4 1.3 copy.21
  379.7 30.2 %all-gather.20.cloned.1.call-done = bf16[2048,512]{1,0:T(8,128)(2,1)} async-done(((bf16[512,512]{1,0:T(8,128)(2,1)}), bf16[2048,512]{1,0:T(8,128)(2,1)}) %all-gather.20.cloned.1.call-update) | async-done | bytes 2097168 | tf_op jit(solution)/shard_map/all_gather | solution.py:73
  409.9 46.1 %all-gather.24.cloned.1.call-done = bf16[512,2048]{1,0:T(8,128)(2,1)} async-done(((bf16[512,512]{1,0:T(8,128)(2,1)}), bf16[512,2048]{1,0:T(8,128)(2,1)}) %all-gather.24.cloned.1.call-update) | async-done | bytes 2097168 | tf_op jit(solution)/shard_map/all_gather | solution.py:96
  456.0 6.5 %convolution_convert_fusion.2 = bf16[512,2048]{1,0:T(8,128)(2,1)} fusion(bf16[512,2048]{1,0:T(8,128)(2,1)} %all-gather.24.cloned.1.call-done, f32[64,8,4,128]{3,2,1,0:T(4,128)} %bitcast.25, bf16[2048,512]{1,0:T(8,128)(2,1)} %all-gather.20.cloned.1.call-done, bf16[512,2048]{1,0:T(8,128)(2,1)S(1)} %copy-done.3, f32[2048]{0:T(1024)S(1)} %copy-done.11, ...), kind=kOutput, calls=%fused_computation.17 | convolution fusion | flops 2155347968 | bytes 9447424 | tf_op jit(solution)/shard_map/dot_general | solution.py:94
  462.5 0.0 reduce-scatter.6.cloned.1.call-update
  462.5 0.0 copy-start.12
  462.5 0.0 all-gather.26.cloned.1.call-start
  462.6 30.1 %reduce-scatter.6.cloned.1.call-done = bf16[128,2048]{1,0:T(8,128)(2,1)} async-done(((bf16[512,2048]{1,0:T(8,128)(2,1)}), bf16[128,2048]{1,0:T(8,128)(2,1)}) %reduce-scatter.6.cloned.1.call-update) | async-done | bytes 524304 | tf_op jit(solution)/shard_map/reduce_scatter | solution.py:99
  492.7 2.0 add_convert_fusion.1
  494.6 0.0 all-gather.26.cloned.1.call-update
  494.6 0.2 reduce-scatter.8.cloned.1.call-start
  494.9 22.5 %all-gather.26.cloned.1.call-done = bf16[512,2048]{1,0:T(8,128)(2,1)} async-done(((bf16[128,2048]{1,0:T(8,128)(2,1)}), bf16[512,2048]{1,0:T(8,128)(2,1)}) %all-gather.26.cloned.1.call-update) | async-done | bytes 2097168 | tf_op jit(solution)/shard_map/all_gather | solution.py:20
  517.4 2.2 fusion.6
  519.6 0.0 copy-done.12
  519.6 5.7 fusion.28
  525.3 9.7 %convolution_convert_fusion = bf16[512,2048]{1,0:T(8,128)(2,1)} fusion(bf16[896,2048]{1,0:T(8,128)(2,1)} %all-gather.16.cloned.1.call-done, f32[512,896]{1,0:T(8,128)} %fusion.28, bf16[2048,896]{1,0:T(8,128)(2,1)} %all-gather.14.cloned.1.call-done, bf16[512,2048]{1,0:T(8,128)(2,1)S(1)} %copy-done.5, f32[2048]{0:T(1024)S(1)} %copy-done.12, ...), kind=kOutput, calls=%fused_computation.15 | convolution fusion | flops 3766091776 | bytes 13379584 | tf_op jit(solution)/shard_map/dot_general | solution.py:45
  535.0 0.0 reduce-scatter.8.cloned.1.call-update
  535.0 31.3 %reduce-scatter.8.cloned.1.call-done = bf16[128,2048]{1,0:T(8,128)(2,1)} async-done(((bf16[512,2048]{1,0:T(8,128)(2,1)}), bf16[128,2048]{1,0:T(8,128)(2,1)}) %reduce-scatter.8.cloned.1.call-update) | async-done | bytes 524304 | tf_op jit(solution)/shard_map/reduce_scatter | solution.py:50
  566.4 2.0 add_convert_fusion
  (20 shorter events, 0.1 us)
Async XLA Ops:
  6.5 27.7 %all-gather.10.cloned.1.call-start = ((), (), s32[]{:S(2)}) async-start(), calls=%async_computation.3 | async-start | bytes 2621440 | tf_op jit(solution)/shard_map/all_gather | solution.py:20
  7.3 100.6 %all-gather.12.cloned.1.call-start = ((), (), s32[]{:S(2)}) async-start(), calls=%async_computation.4 | async-start | bytes 4587520 | tf_op jit(solution)/shard_map/all_gather | solution.py:40
  8.0 99.9 %copy-start.10 = (f32[2048]{0:T(1024)S(1)}, f32[2048]{0:T(1024)}, u32[]{:S(2)}) copy-start(f32[2048]{0:T(1024)} %param.15) | copy-start | bytes 24580
  8.0 172.2 %all-gather.14.cloned.1.call-start = ((), (), s32[]{:S(2)}) async-start(), calls=%async_computation.5 | async-start | bytes 4587520 | tf_op jit(solution)/shard_map/all_gather | solution.py:41
  8.8 243.5 %all-gather.16.cloned.1.call-start = ((), (), s32[]{:S(2)}) async-start(), calls=%async_computation.6 | async-start | bytes 4587520 | tf_op jit(solution)/shard_map/all_gather | solution.py:47
  9.3 282.6 %reduce-scatter.4.cloned.1.call-start = ((), (), s32[]{:S(2)}) async-start(), calls=%async_computation.7 | async-start | bytes 2621440 | tf_op jit(solution)/shard_map/reduce_scatter | solution.py:50
  34.2 73.7 %copy-start.4 = (bf16[512,2048]{1,0:T(8,128)(2,1)S(1)}, bf16[512,2048]{1,0:T(8,128)(2,1)}, u32[]{:S(2)}) copy-start(bf16[512,2048]{1,0:T(8,128)(2,1)} %all-gather.10.cloned.1.call-done) | copy-start | bytes 6291460
  262.0 29.9 %copy-start.2 = (bf16[128,2048]{1,0:T(8,128)(2,1)S(1)}, bf16[128,2048]{1,0:T(8,128)(2,1)}, u32[]{:S(2)}) copy-start(bf16[128,2048]{1,0:T(8,128)(2,1)} %param.14) | copy-start | bytes 1572868
  262.0 54.6 %all-gather.18.cloned.1.call-start = ((), (), s32[]{:S(2)}) async-start(), calls=%async_computation.8 | async-start | bytes 2621440 | tf_op jit(solution)/shard_map/all_gather | solution.py:67
  293.9 70.0 %copy-start.11 = (f32[2048]{0:T(1024)S(1)}, f32[2048]{0:T(1024)}, u32[]{:S(2)}) copy-start(f32[2048]{0:T(1024)} %param.20) | copy-start | bytes 24580
  293.9 70.0 %all-gather.22.cloned.1.call-start = ((), (), s32[]{:S(2)}) async-start(), calls=%async_computation.10 | async-start | bytes 2621440 | tf_op jit(solution)/shard_map/all_gather | solution.py:74
  294.7 115.3 %all-gather.20.cloned.1.call-start = ((), (), s32[]{:S(2)}) async-start(), calls=%async_computation.9 | async-start | bytes 2621440 | tf_op jit(solution)/shard_map/all_gather | solution.py:73
  295.4 160.6 %all-gather.24.cloned.1.call-start = ((), (), s32[]{:S(2)}) async-start(), calls=%async_computation.11 | async-start | bytes 2621440 | tf_op jit(solution)/shard_map/all_gather | solution.py:96
  296.2 196.5 %reduce-scatter.6.cloned.1.call-start = ((), (), s32[]{:S(2)}) async-start(), calls=%async_computation.12 | async-start | bytes 2621440 | tf_op jit(solution)/shard_map/reduce_scatter | solution.py:99
  316.6 47.3 %copy-start.3 = (bf16[512,2048]{1,0:T(8,128)(2,1)S(1)}, bf16[512,2048]{1,0:T(8,128)(2,1)}, u32[]{:S(2)}) copy-start(bf16[512,2048]{1,0:T(8,128)(2,1)} %all-gather.18.cloned.1.call-done) | copy-start | bytes 6291460
  318.9 55.7 %copy-start.7 = (f32[512]{0:T(512)S(1)}, f32[512]{0:T(512)}, u32[]{:S(2)}) copy-start(f32[512]{0:T(512)} %param.24) | copy-start | bytes 6148
  318.9 55.7 %copy-start.8 = (f32[512]{0:T(512)S(1)}, f32[512]{0:T(512)}, u32[]{:S(2)}) copy-start(f32[512]{0:T(512)} %param.23) | copy-start | bytes 6148
  368.0 8.9 %copy-start.6 = (bf16[4,128,128]{2,1,0:T(8,128)(2,1)S(1)}, bf16[4,128,128]{2,1,0:T(8,128)(2,1)}, u32[]{:S(2)}) copy-start(bf16[4,128,128]{2,1,0:T(8,128)(2,1)} %param.25) | copy-start | bytes 393220
  368.0 8.9 %copy-start.9 = (f32[4,128]{1,0:T(4,128)S(1)}, f32[4,128]{1,0:T(4,128)}, u32[]{:S(2)}) copy-start(f32[4,128]{1,0:T(4,128)} %param.26) | copy-start | bytes 6148
  462.5 30.2 %copy-start = (bf16[128,2048]{1,0:T(8,128)(2,1)S(1)}, bf16[128,2048]{1,0:T(8,128)(2,1)}, u32[]{:S(2)}) copy-start(bf16[128,2048]{1,0:T(8,128)(2,1)} %add_convert_fusion.3) | copy-start | bytes 1572868
  462.5 57.1 %copy-start.12 = (f32[2048]{0:T(1024)S(1)}, f32[2048]{0:T(1024)}, u32[]{:S(2)}) copy-start(f32[2048]{0:T(1024)} %param.16) | copy-start | bytes 24580
  462.5 54.8 %all-gather.26.cloned.1.call-start = ((), (), s32[]{:S(2)}) async-start(), calls=%async_computation.13 | async-start | bytes 2621440 | tf_op jit(solution)/shard_map/all_gather | solution.py:20
  494.6 71.7 %reduce-scatter.8.cloned.1.call-start = ((), (), s32[]{:S(2)}) async-start(), calls=%async_computation.14 | async-start | bytes 2621440 | tf_op jit(solution)/shard_map/reduce_scatter | solution.py:50
  517.4 2.2 copy-start.5
  535.0 31.4 %copy-start.1 = (bf16[128,2048]{1,0:T(8,128)(2,1)S(1)}, bf16[128,2048]{1,0:T(8,128)(2,1)}, u32[]{:S(2)}) copy-start(bf16[128,2048]{1,0:T(8,128)(2,1)} %add_convert_fusion.1) | copy-start | bytes 1572868
Sparse Core Ops, SparseCore 0:
  8.9 25.2 all-gather.9
  35.8 72.0 all-gather.11
  109.5 70.6 all-gather.13
  181.6 70.6 all-gather.15
  262.1 29.7 reduce-scatter.3
  294.1 22.5 all-gather.17
  318.2 45.6 all-gather.21
  365.5 44.4 all-gather.19
  411.5 44.4 all-gather.23
  462.6 29.9 reduce-scatter.5
  494.8 22.5 all-gather.25
  535.1 31.1 reduce-scatter.7
where the time goes:
time: 576 us; the launch traced here: 575 us
  waiting for transfers between devices  495 us (86%)
  matrix products  42.7 us (7%)
  other arithmetic  14.1 us (2%)
  between operations  13.7 us (2%)
  blocking collectives  6.51 us (1%)
    all_gather x1, waiting for transfers between devices, half_again(): lax.all_gather(proj_down, 'fs', axis=1, tiled=True)  72.1 us
    all_gather x1, waiting for transfers between devices, half_again(): lax.all_gather(proj_gate, 'fs', axis=0, tiled=True)  71.5 us
    all_gather x1, waiting for transfers between devices, half_again(): lax.all_gather(proj_lift, 'fs', axis=0, tiled=True)  66.6 us
    reduce_scatter x2, waiting for transfers between devices, half_again(): lax.psum_scatter(partial_value.astype(jnp.bfloat16), 'tp', scatter_dimens...  61.2 us
    all_gather x2, waiting for transfers between devices, gathered_norm(): gathered = lax.all_gather(stream_rows, 'tp', axis=0, tiled=True)  47.3 us
    all_gather x1, waiting for transfers between devices, token_mixer(): lax.all_gather(mixer_down, 'fs', axis=1, tiled=True)  46.1 us
    all_gather x1, waiting for transfers between devices, token_mixer(): lax.all_gather(mixer_v, 'fs', axis=0, tiled=True)  45 us
    all_gather x1, waiting for transfers between devices, token_mixer(): lax.all_gather(mixer_u, 'fs', axis=0, tiled=True)  30.2 us
  transfers between devices with their start and end apart: 12, of which 12 were waited for; matrix products, arithmetic and copies ran while one was open for 3% of the time, Pallas kernels for 0%

commit v1 on v0

--- a/solution.py
+++ b/solution.py
@@ -1,3 +1,4 @@
+import functools
 import jax
 import jax.numpy as jnp
 from jax import lax
@@ -10,6 +11,21 @@
 layer_epsilon = 1e-05
 
 
+def bring_heaps(x_in, lane_axis):
+    parts_n = lax.axis_size(lane_axis)
+    by_place = [(c, (c + 1) % parts_n) for c in range(parts_n)]
+    s_next = [None] * parts_n
+    s_next[parts_n - 1] = x_in
+    for u in range(parts_n - 2, -1, -1):
+        s_next[u] = lax.ppermute(s_next[u + 1], lane_axis, perm=by_place)
+    left_arr = jnp.concatenate(s_next, axis=0)
+    later = (lax.axis_index(lane_axis) + 1) * x_in.shape[0]
+    return jnp.roll(left_arr, later, axis=0)
+
+
+point_table = functools.partial(bring_heaps, lane_axis="tp")
+
+
 def norm_rows(row_block, scale_gain):
     widened = row_block.astype(jnp.float32)
     factor = lax.rsqrt(jnp.mean(widened * widened, axis=1, keepdims=True) + norm_epsilon)
@@ -17,7 +33,7 @@
 
 
 def gathered_norm(stream_rows, scale_gain):
-    gathered = lax.all_gather(stream_rows, "tp", axis=0, tiled=True)
+    gathered = point_table(stream_rows)
     return norm_rows(gathered, scale_gain)
 
 

time: 576 us -> 553 us (0.960)
  waiting for transfers between devices: 495 us -> 471 us
    ppermute x0 -> x6, waiting for transfers between devices: none -> 52.1 us  [bring_heaps(): s_next[u] = lax.ppermute(s_next[u + 1], lane_axis, perm=by_place)]
    all_gather x2 -> x0, waiting for transfers between devices: 47.3 us -> none  [gathered_norm(): gathered = lax.all_gather(stream_rows, 'tp', axis=0, tiled=True)]
    all_gather x1, waiting for transfers between devices: 71.5 us -> 43.7 us  [half_again(): lax.all_gather(proj_gate, 'fs', axis=0, tiled=True)]
  transfers between devices with their start and end apart: 12 -> 16, of which waited for: 12 -> 16; matrix products, arithmetic and copies ran while one was open for 3% -> 4% of each run, Pallas kernels for 0% -> 0%
where the time goes in v1:
time: 553 us
  waiting for transfers between devices  471 us (85%)
  matrix products  41.4 us (7%)
  other arithmetic  16.9 us (3%)
  between operations  13.7 us (2%)
  blocking collectives  6.68 us (1%)
    all_gather x1, waiting for transfers between devices, half_again(): lax.all_gather(proj_down, 'fs', axis=1, tiled=True)  72.3 us
    all_gather x1, waiting for transfers between devices, half_again(): lax.all_gather(proj_lift, 'fs', axis=0, tiled=True)  66.6 us
    reduce_scatter x2, waiting for transfers between devices, half_again(): lax.psum_scatter(partial_value.astype(jnp.bfloat16), 'tp', scatter_dimens...  61.1 us
    ppermute x6, waiting for transfers between devices, bring_heaps(): s_next[u] = lax.ppermute(s_next[u + 1], lane_axis, perm=by_place)  52.1 us
    all_gather x1, waiting for transfers between devices, token_mixer(): lax.all_gather(mixer_down, 'fs', axis=1, tiled=True)  46.1 us
    all_gather x1, waiting for transfers between devices, token_mixer(): lax.all_gather(mixer_v, 'fs', axis=0, tiled=True)  45 us
    all_gather x1, waiting for transfers between devices, half_again(): lax.all_gather(proj_gate, 'fs', axis=0, tiled=True)  43.7 us
    reduce_scatter x1, waiting for transfers between devices, token_mixer(): lax.psum_scatter(partial_value.astype(jnp.bfloat16), 'tp', scatter_dimens...  30.1 us
  transfers between devices with their start and end apart: 16, of which 16 were waited for; matrix products, arithmetic and copies ran while one was open for 4% of the time, Pallas kernels for 0%

profile of v1, /device:TPU:0, one launch (start us, length us, event | category | flops | bytes accessed | tf_op | source)
XLA Modules:
  0.0 553.0 jit_solution(13497951438309852413)
XLA Ops:
  6.5 0.7 all-gather.8.cloned.1.call-update
  7.3 0.0 all-gather.10.cloned.1.call-start
  7.3 0.7 all-gather.10.cloned.1.call-update
  8.0 0.0 all-gather.12.cloned.1.call-start
  8.1 0.7 all-gather.12.cloned.1.call-update
  8.7 0.0 reduce-scatter.4.cloned.1.call-start
  8.8 0.5 collective-permute-start
  9.3 9.0 %collective-permute-done = bf16[128,2048]{1,0:T(8,128)(2,1)S(1)} collective-permute-done((bf16[128,2048]{1,0:T(8,128)(2,1)}, bf16[128,2048]{1,0:T(8,128)(2,1)S(1)}, u32[]{:S(2)}, u32[]{:S(2)}) %collective-permute-start) | collective-permute-done | bytes 524320 | tf_op jit(solution)/shard_map/ppermute | solution.py:20
  18.3 0.0 collective-permute-start.1
  18.4 8.6 %collective-permute-done.1 = bf16[128,2048]{1,0:T(8,128)(2,1)S(1)} collective-permute-done((bf16[128,2048]{1,0:T(8,128)(2,1)S(1)}, bf16[128,2048]{1,0:T(8,128)(2,1)S(1)}, u32[]{:S(2)}, u32[]{:S(2)}) %collective-permute-start.1) | collective-permute-done | bytes 524320 | tf_op jit(solution)/shard_map/ppermute | solution.py:20
  26.9 0.0 collective-permute-start.2
  26.9 8.7 %collective-permute-done.2 = bf16[128,2048]{1,0:T(8,128)(2,1)} collective-permute-done((bf16[128,2048]{1,0:T(8,128)(2,1)S(1)}, bf16[128,2048]{1,0:T(8,128)(2,1)}, u32[]{:S(2)}, u32[]{:S(2)}) %collective-permute-start.2) | collective-permute-done | bytes 524320 | tf_op jit(solution)/shard_map/ppermute | solution.py:20
  35.6 4.4 fusion
  40.1 43.7 %all-gather.8.cloned.1.call-done = bf16[2048,896]{1,0:T(8,128)(2,1)} async-done(((bf16[512,896]{1,0:T(8,128)(2,1)}), bf16[2048,896]{1,0:T(8,128)(2,1)}) %all-gather.8.cloned.1.call-update) | async-done | bytes 3670032 | tf_op jit(solution)/shard_map/all_gather | solution.py:56
  83.8 5.6 %fusion.56 = f32[512,896]{1,0:T(8,128)} fusion(bf16[2048,896]{1,0:T(8,128)(2,1)} %all-gather.8.cloned.1.call-done, bf16[512,2048]{1,0:T(8,128)(2,1)S(1)} %get-tuple-element.13, f32[2048]{0:T(1024)S(1)} %copy-done.8, f32[512]{0:T(512)S(1)} %add_rsqrt_fusion.3), kind=kOutput, calls=%fused_computation.78 | convolution fusion | flops 1883242496 | bytes 7612416 | tf_op jit(solution)/shard_map/dot_general | solution.py:42
  89.4 66.6 %all-gather.10.cloned.1.call-done = bf16[2048,896]{1,0:T(8,128)(2,1)} async-done(((bf16[512,896]{1,0:T(8,128)(2,1)}), bf16[2048,896]{1,0:T(8,128)(2,1)}) %all-gather.10.cloned.1.call-update) | async-done | bytes 3670032 | tf_op jit(solution)/shard_map/all_gather | solution.py:57
  156.0 72.3 %all-gather.12.cloned.1.call-done = bf16[896,2048]{1,0:T(8,128)(2,1)} async-done(((bf16[896,512]{1,0:T(8,128)(2,1)}), bf16[896,2048]{1,0:T(8,128)(2,1)}) %all-gather.12.cloned.1.call-update) | async-done | bytes 3670032 | tf_op jit(solution)/shard_map/all_gather | solution.py:63
  228.3 9.7 %convolution_convert_fusion.1 = bf16[512,2048]{1,0:T(8,128)(2,1)} fusion(bf16[896,2048]{1,0:T(8,128)(2,1)} %all-gather.12.cloned.1.call-done, f32[512,896]{1,0:T(8,128)} %fusion.56, bf16[2048,896]{1,0:T(8,128)(2,1)} %all-gather.10.cloned.1.call-done, bf16[512,2048]{1,0:T(8,128)(2,1)S(1)} %get-tuple-element.13, f32[2048]{0:T(1024)S(1)} %copy-done.8, ...), kind=kOutput, calls=%fused_computation.32 | convolution fusion | flops 3766091776 | bytes 13379584 | tf_op jit(solution)/shard_map/dot_general | solution.py:61
  238.0 0.0 reduce-scatter.4.cloned.1.call-update
  238.0 0.0 all-gather.14.cloned.1.call-start
  238.0 29.8 %reduce-scatter.4.cloned.1.call-done = bf16[128,2048]{1,0:T(8,128)(2,1)} async-done(((bf16[512,2048]{1,0:T(8,128)(2,1)}), bf16[128,2048]{1,0:T(8,128)(2,1)}) %reduce-scatter.4.cloned.1.call-update) | async-done | bytes 524304 | tf_op jit(solution)/shard_map/reduce_scatter | solution.py:66
  267.9 2.0 add_convert_fusion.3
  269.9 0.0 all-gather.14.cloned.1.call-update
  269.9 0.0 all-gather.18.cloned.1.call-start
  269.9 0.5 all-gather.18.cloned.1.call-update
  270.5 0.0 all-gather.16.cloned.1.call-start
  270.5 0.7 all-gather.16.cloned.1.call-update
  271.2 0.0 all-gather.20.cloned.1.call-start
  271.3 0.7 all-gather.20.cloned.1.call-update
  272.0 0.0 reduce-scatter.6.cloned.1.call-start
  272.0 20.6 %all-gather.14.cloned.1.call-done = bf16[512,2048]{1,0:T(8,128)(2,1)} async-done(((bf16[128,2048]{1,0:T(8,128)(2,1)}), bf16[512,2048]{1,0:T(8,128)(2,1)}) %all-gather.14.cloned.1.call-update) | async-done | bytes 2097168 | tf_op jit(solution)/shard_map/all_gather | solution.py:83
  292.6 2.1 fusion.3
  294.7 0.0 copy-start.4
  294.7 0.0 copy-start.5
  294.7 0.0 copy-start.3
  294.7 0.0 copy-start.6
  294.7 45.0 %all-gather.18.cloned.1.call-done = bf16[2048,512]{1,0:T(8,128)(2,1)} async-done(((bf16[512,512]{1,0:T(8,128)(2,1)}), bf16[2048,512]{1,0:T(8,128)(2,1)}) %all-gather.18.cloned.1.call-update) | async-done | bytes 2097168 | tf_op jit(solution)/shard_map/all_gather | solution.py:90
  339.7 4.7 fusion.74
  344.5 6.7 %all-reduce = (f32[512]{0:T(512)S(1)}, f32[512]{0:T(512)S(1)}) all-reduce(f32[512]{0:T(512)S(1)} %get-tuple-element.7, f32[512]{0:T(512)S(1)} %get-tuple-element.6), channel_id=1, replica_groups=mesh['rep'=2,'fs'=4,'tp'=4] {'tp'}, use_global_device_ids=true, to_apply=%region_6.8 | all-reduce | flops 1024 | bytes 8192 | tf_op jit(solution)/shard_map/psum | solution.py:94
  351.2 0.0 copy-done.4
  351.2 1.5 add_convert_fusion.2
  352.6 0.9 reshape.47
  353.6 0.0 copy-done.6
  353.6 1.4 fusion.23
  355.0 1.3 copy.21
  356.3 29.5 %all-gather.16.cloned.1.call-done = bf16[2048,512]{1,0:T(8,128)(2,1)} async-done(((bf16[512,512]{1,0:T(8,128)(2,1)}), bf16[2048,512]{1,0:T(8,128)(2,1)}) %all-gather.16.cloned.1.call-update) | async-done | bytes 2097168 | tf_op jit(solution)/shard_map/all_gather | solution.py:89
  385.8 46.1 %all-gather.20.cloned.1.call-done = bf16[512,2048]{1,0:T(8,128)(2,1)} async-done(((bf16[512,512]{1,0:T(8,128)(2,1)}), bf16[512,2048]{1,0:T(8,128)(2,1)}) %all-gather.20.cloned.1.call-update) | async-done | bytes 2097168 | tf_op jit(solution)/shard_map/all_gather | solution.py:112
  431.9 6.6 %convolution_convert_fusion.2 = bf16[512,2048]{1,0:T(8,128)(2,1)} fusion(bf16[512,2048]{1,0:T(8,128)(2,1)} %all-gather.20.cloned.1.call-done, f32[64,8,4,128]{3,2,1,0:T(4,128)} %bitcast.25, bf16[2048,512]{1,0:T(8,128)(2,1)} %all-gather.16.cloned.1.call-done, bf16[512,2048]{1,0:T(8,128)(2,1)S(1)} %copy-done.1, f32[2048]{0:T(1024)S(1)} %copy-done.9, ...), kind=kOutput, calls=%fused_computation.33 | convolution fusion | flops 2155347968 | bytes 9447424 | tf_op jit(solution)/shard_map/dot_general | solution.py:110
  438.5 0.0 reduce-scatter.6.cloned.1.call-update
  438.5 0.0 reduce-scatter.8.cloned.1.call-start
  438.6 30.1 %reduce-scatter.6.cloned.1.call-done = bf16[128,2048]{1,0:T(8,128)(2,1)} async-done(((bf16[512,2048]{1,0:T(8,128)(2,1)}), bf16[128,2048]{1,0:T(8,128)(2,1)}) %reduce-scatter.6.cloned.1.call-update) | async-done | bytes 524304 | tf_op jit(solution)/shard_map/reduce_scatter | solution.py:115
  468.7 1.3 add_convert_fusion.1
  470.0 0.1 collective-permute-start.3
  470.0 8.6 %collective-permute-done.3 = bf16[128,2048]{1,0:T(8,128)(2,1)S(1)} collective-permute-done((bf16[128,2048]{1,0:T(8,128)(2,1)S(1)}, bf16[128,2048]{1,0:T(8,128)(2,1)S(1)}, u32[]{:S(2)}, u32[]{:S(2)}) %collective-permute-start.3) | collective-permute-done | bytes 524320 | tf_op jit(solution)/shard_map/ppermute | solution.py:20
  478.6 0.0 collective-permute-start.4
  478.6 8.6 %collective-permute-done.4 = bf16[128,2048]{1,0:T(8,128)(2,1)S(1)} collective-permute-done((bf16[128,2048]{1,0:T(8,128)(2,1)S(1)}, bf16[128,2048]{1,0:T(8,128)(2,1)S(1)}, u32[]{:S(2)}, u32[]{:S(2)}) %collective-permute-start.4) | collective-permute-done | bytes 524320 | tf_op jit(solution)/shard_map/ppermute | solution.py:20
  487.2 0.0 collective-permute-start.5
  487.2 8.6 %collective-permute-done.5 = bf16[128,2048]{1,0:T(8,128)(2,1)S(1)} collective-permute-done((bf16[128,2048]{1,0:T(8,128)(2,1)S(1)}, bf16[128,2048]{1,0:T(8,128)(2,1)S(1)}, u32[]{:S(2)}, u32[]{:S(2)}) %collective-permute-start.5) | collective-permute-done | bytes 524320 | tf_op jit(solution)/shard_map/ppermute | solution.py:20
  495.9 3.6 fusion.6
  499.5 3.6 fusion.42
  503.2 9.7 %convolution_convert_fusion = bf16[512,2048]{1,0:T(8,128)(2,1)} fusion(bf16[896,2048]{1,0:T(8,128)(2,1)} %all-gather.12.cloned.1.call-done, f32[512,896]{1,0:T(8,128)} %fusion.42, bf16[2048,896]{1,0:T(8,128)(2,1)} %all-gather.10.cloned.1.call-done, bf16[512,2048]{1,0:T(8,128)(2,1)S(1)} %get-tuple-element.11, f32[2048]{0:T(1024)S(1)} %copy-done.10, ...), kind=kOutput, calls=%fused_computation.31 | convolution fusion | flops 3766091776 | bytes 13379584 | tf_op jit(solution)/shard_map/dot_general | solution.py:61
  512.9 0.0 reduce-scatter.8.cloned.1.call-update
  512.9 31.3 %reduce-scatter.8.cloned.1.call-done = bf16[128,2048]{1,0:T(8,128)(2,1)} async-done(((bf16[512,2048]{1,0:T(8,128)(2,1)}), bf16[128,2048]{1,0:T(8,128)(2,1)}) %reduce-scatter.8.cloned.1.call-update) | async-done | bytes 524304 | tf_op jit(solution)/shard_map/reduce_scatter | solution.py:66
  544.2 2.0 add_convert_fusion
  (22 shorter events, 0.1 us)
Async XLA Ops:
  6.5 77.2 %copy-start.8 = (f32[2048]{0:T(1024)S(1)}, f32[2048]{0:T(1024)}, u32[]{:S(2)}) copy-start(f32[2048]{0:T(1024)} %param.17) | copy-start | bytes 24580
  6.5 77.2 %all-gather.8.cloned.1.call-start = ((), (), s32[]{:S(2)}) async-start(), calls=%async_computation.3 | async-start | bytes 4587520 | tf_op jit(solution)/shard_map/all_gather | solution.py:56
  7.3 148.8 %all-gather.10.cloned.1.call-start = ((), (), s32[]{:S(2)}) async-start(), calls=%async_computation.4 | async-start | bytes 4587520 | tf_op jit(solution)/shard_map/all_gather | solution.py:57
  8.0 220.3 %all-gather.12.cloned.1.call-start = ((), (), s32[]{:S(2)}) async-start(), calls=%async_computation.5 | async-start | bytes 4587520 | tf_op jit(solution)/shard_map/all_gather | solution.py:63
  8.7 259.1 %reduce-scatter.4.cloned.1.call-start = ((), (), s32[]{:S(2)}) async-start(), calls=%async_computation.6 | async-start | bytes 2621440 | tf_op jit(solution)/shard_map/reduce_scatter | solution.py:66
  8.8 9.5 %collective-permute-start = (bf16[128,2048]{1,0:T(8,128)(2,1)}, bf16[128,2048]{1,0:T(8,128)(2,1)S(1)}, u32[]{:S(2)}, u32[]{:S(2)}) collective-permute-start(bf16[128,2048]{1,0:T(8,128)(2,1)} %param.16), channel_id=1, source_target_pairs={{0,1},{1,2},{2,3},{3,0},{4,5},{5,6},{6,7},{7,4},{8,9},{9,10},{10,1... | collective-permute-start | bytes 1572872 | tf_op jit(solution)/shard_map/ppermute | solution.py:20
  18.3 8.6 %collective-permute-start.1 = (bf16[128,2048]{1,0:T(8,128)(2,1)S(1)}, bf16[128,2048]{1,0:T(8,128)(2,1)S(1)}, u32[]{:S(2)}, u32[]{:S(2)}) collective-permute-start(bf16[128,2048]{1,0:T(8,128)(2,1)S(1)} %collective-permute-done), channel_id=1, source_target_pairs={{0,1},{1,2},{2,3},{3,0},{4,5},{5,6},{6,7},{7,4},{8,9},{9,10},{10,1... | collective-permute-start | bytes 1572872 | tf_op jit(solution)/shard_map/ppermute | solution.py:20
  26.9 8.7 %collective-permute-start.2 = (bf16[128,2048]{1,0:T(8,128)(2,1)S(1)}, bf16[128,2048]{1,0:T(8,128)(2,1)}, u32[]{:S(2)}, u32[]{:S(2)}) collective-permute-start(bf16[128,2048]{1,0:T(8,128)(2,1)S(1)} %collective-permute-done.1), channel_id=1, source_target_pairs={{0,1},{1,2},{2,3},{3,0},{4,5},{5,6},{6,7},{7,4},{8,9},{9,10},{10,1... | collective-permute-start | bytes 1572872 | tf_op jit(solution)/shard_map/ppermute | solution.py:20
  89.4 178.5 %copy-start.2 = (bf16[128,2048]{1,0:T(8,128)(2,1)S(1)}, bf16[128,2048]{1,0:T(8,128)(2,1)}, u32[]{:S(2)}) copy-start(bf16[128,2048]{1,0:T(8,128)(2,1)} %param.16) | copy-start | bytes 1572868
  238.0 101.8 %copy-start.9 = (f32[2048]{0:T(1024)S(1)}, f32[2048]{0:T(1024)}, u32[]{:S(2)}) copy-start(f32[2048]{0:T(1024)} %param.22) | copy-start | bytes 24580
  238.0 54.6 %all-gather.14.cloned.1.call-start = ((), (), s32[]{:S(2)}) async-start(), calls=%async_computation.7 | async-start | bytes 2621440 | tf_op jit(solution)/shard_map/all_gather | solution.py:83
  269.9 69.8 %all-gather.18.cloned.1.call-start = ((), (), s32[]{:S(2)}) async-start(), calls=%async_computation.9 | async-start | bytes 2621440 | tf_op jit(solution)/shard_map/all_gather | solution.py:90
  270.5 115.3 %all-gather.16.cloned.1.call-start = ((), (), s32[]{:S(2)}) async-start(), calls=%async_computation.8 | async-start | bytes 2621440 | tf_op jit(solution)/shard_map/all_gather | solution.py:89
  271.2 160.6 %all-gather.20.cloned.1.call-start = ((), (), s32[]{:S(2)}) async-start(), calls=%async_computation.10 | async-start | bytes 2621440 | tf_op jit(solution)/shard_map/all_gather | solution.py:112
  272.0 196.7 %reduce-scatter.6.cloned.1.call-start = ((), (), s32[]{:S(2)}) async-start(), calls=%async_computation.11 | async-start | bytes 2621440 | tf_op jit(solution)/shard_map/reduce_scatter | solution.py:115
  294.7 56.5 %copy-start.4 = (f32[512]{0:T(512)S(1)}, f32[512]{0:T(512)}, u32[]{:S(2)}) copy-start(f32[512]{0:T(512)} %param.26) | copy-start | bytes 6148
  294.7 56.5 %copy-start.5 = (f32[512]{0:T(512)S(1)}, f32[512]{0:T(512)}, u32[]{:S(2)}) copy-start(f32[512]{0:T(512)} %param.25) | copy-start | bytes 6148
  294.7 58.8 %copy-start.3 = (bf16[4,128,128]{2,1,0:T(8,128)(2,1)S(1)}, bf16[4,128,128]{2,1,0:T(8,128)(2,1)}, u32[]{:S(2)}) copy-start(bf16[4,128,128]{2,1,0:T(8,128)(2,1)} %param.27) | copy-start | bytes 393220
  294.7 58.8 %copy-start.6 = (f32[4,128]{1,0:T(4,128)S(1)}, f32[4,128]{1,0:T(4,128)}, u32[]{:S(2)}) copy-start(f32[4,128]{1,0:T(4,128)} %param.28) | copy-start | bytes 6148
  344.5 87.4 %copy-start.1 = (bf16[512,2048]{1,0:T(8,128)(2,1)S(1)}, bf16[512,2048]{1,0:T(8,128)(2,1)}, u32[]{:S(2)}) copy-start(bf16[512,2048]{1,0:T(8,128)(2,1)} %all-gather.14.cloned.1.call-done) | copy-start | bytes 6291460
  431.9 36.8 %copy-start = (bf16[128,2048]{1,0:T(8,128)(2,1)S(1)}, bf16[128,2048]{1,0:T(8,128)(2,1)}, u32[]{:S(2)}) copy-start(bf16[128,2048]{1,0:T(8,128)(2,1)} %add_convert_fusion.3) | copy-start | bytes 1572868
  438.5 61.0 %copy-start.10 = (f32[2048]{0:T(1024)S(1)}, f32[2048]{0:T(1024)}, u32[]{:S(2)}) copy-start(f32[2048]{0:T(1024)} %param.18) | copy-start | bytes 24580
  438.5 105.7 %reduce-scatter.8.cloned.1.call-start = ((), (), s32[]{:S(2)}) async-start(), calls=%async_computation.12 | async-start | bytes 2621440 | tf_op jit(solution)/shard_map/reduce_scatter | solution.py:66
  468.7 30.9 %copy-start.7 = (bf16[2048,896]{1,0:T(8,128)(2,1)S(1)}, bf16[2048,896]{1,0:T(8,128)(2,1)}, u32[]{:S(2)}) copy-start(bf16[2048,896]{1,0:T(8,128)(2,1)} %all-gather.8.cloned.1.call-done) | copy-start | bytes 11010052
  470.0 8.7 %collective-permute-start.3 = (bf16[128,2048]{1,0:T(8,128)(2,1)S(1)}, bf16[128,2048]{1,0:T(8,128)(2,1)S(1)}, u32[]{:S(2)}, u32[]{:S(2)}) collective-permute-start(bf16[128,2048]{1,0:T(8,128)(2,1)S(1)} %add_convert_fusion.1), channel_id=1, source_target_pairs={{0,1},{1,2},{2,3},{3,0},{4,5},{5,6},{6,7},{7,4},{8,9},{9,10},{10,1... | collective-permute-start | bytes 1572872 | tf_op jit(solution)/shard_map/ppermute | solution.py:20
  478.6 8.6 %collective-permute-start.4 = (bf16[128,2048]{1,0:T(8,128)(2,1)S(1)}, bf16[128,2048]{1,0:T(8,128)(2,1)S(1)}, u32[]{:S(2)}, u32[]{:S(2)}) collective-permute-start(bf16[128,2048]{1,0:T(8,128)(2,1)S(1)} %collective-permute-done.3), channel_id=1, source_target_pairs={{0,1},{1,2},{2,3},{3,0},{4,5},{5,6},{6,7},{7,4},{8,9},{9,10},{10,1... | collective-permute-start | bytes 1572872 | tf_op jit(solution)/shard_map/ppermute | solution.py:20
  487.2 8.6 %collective-permute-start.5 = (bf16[128,2048]{1,0:T(8,128)(2,1)S(1)}, bf16[128,2048]{1,0:T(8,128)(2,1)S(1)}, u32[]{:S(2)}, u32[]{:S(2)}) collective-permute-start(bf16[128,2048]{1,0:T(8,128)(2,1)S(1)} %collective-permute-done.4), channel_id=1, source_target_pairs={{0,1},{1,2},{2,3},{3,0},{4,5},{5,6},{6,7},{7,4},{8,9},{9,10},{10,1... | collective-permute-start | bytes 1572872 | tf_op jit(solution)/shard_map/ppermute | solution.py:20
Sparse Core Ops, SparseCore 0:
  8.9 74.8 all-gather.7
  85.3 70.6 all-gather.9
  157.6 70.6 all-gather.11
  238.1 29.7 reduce-scatter.3
  270.0 22.5 all-gather.13
  294.0 45.6 all-gather.17
  341.3 44.4 all-gather.15
  387.4 44.4 all-gather.19
  438.6 29.9 reduce-scatter.5
  513.0 31.1 reduce-scatter.7
